TPU v7x, 32 devices: a whole 2x2x4 slice. The times are simulated.
32 devices in a mesh: sp: 4 (over z), fs: 4 (over y, x), tp: 2 (over core).
Axes of the slice: x: 2, y: 2, z: 4, core: 2. Of those that a mesh axis runs over, the one named last changes fastest.
Arguments:
- inputs: bfloat16 [4, 2048, 2048], P('fs', 'sp', 'tp'), may hold values from -6 to 6
- norm_gain: float32 [2048], replicated, may hold values from 0.1 to 1.9
- query_weight: bfloat16 [2048, 1024], P(('sp', 'fs'), 'tp'), may hold values from -0.125 to 0.125
- key_weight: bfloat16 [2048, 1024], P(('sp', 'fs'), 'tp'), may hold values from -0.125 to 0.125
- value_weight: bfloat16 [2048, 1024], P(('sp', 'fs'), 'tp'), may hold values from -0.125 to 0.125
- query_gain: float32 [64], replicated, may hold values from 0.8 to 7
- key_gain: float32 [64], replicated, may hold values from 0.8 to 7
- mix_lambda: float32 [8], replicated, may hold values from 0.3 to 0.8
- head_gain: float32 [128], replicated, may hold values from 0.1 to 1.9
- post_gate_weight: bfloat16 [2048, 2048], P(('sp', 'fs'), 'tp'), may hold values from -0.125 to 0.125
- pre_gate_weight: bfloat16 [2048, 2048], P(('sp', 'fs'), 'tp'), may hold values from -0.125 to 0.125
- inner_weight: bfloat16 [2048, 2048], P(('sp', 'fs'), 'tp'), may hold values from -0.125 to 0.125
- conv_taps: float32 [3, 2048], replicated, may hold values from -3 to 3
- attn_out_weight: bfloat16 [2048, 1024], P(('sp', 'fs'), 'tp'), may hold values from -0.109375 to 0.109375
- conv_out_weight: bfloat16 [2048, 2048], P(('sp', 'fs'), 'tp'), may hold values from -0.109375 to 0.109375
Outputs:
- mixed: bfloat16 [4, 2048, 2048], P('fs', ('sp', 'tp'))
All inputs are finite; a program needn't handle non-finite values.
Results may differ from a plain program's by a relative error of at most 0.015.
The roundings to bfloat16 on the way count: a program that leaves them out, or rounds other values in their place, can miss the bound.
Values may be sent and summed in bfloat16 or wider, within the bound.
A program may use at most 128 MiB of HBM per device.

v0:
```python
import math
import jax
import jax.numpy as jnp
from jax import lax
from jax.sharding import PartitionSpec as P

epsilon = 1e-06


def padded_2(x, sides, width):
    for axis, dim in sides:
        size, length = (lax.axis_size(axis), x.shape[dim])
        up = [(i, (i + 1) % size) for i in range(size - 1)]
        down = [(j, i) for i, j in up]
        last = lax.slice_in_dim(x, length - width, length, axis=dim)
        initial = lax.slice_in_dim(x, 0, width, axis=dim)
        before = lax.ppermute(last, axis, up)
        after = lax.ppermute(initial, axis, down)
        x = jnp.concatenate([before, x, after], axis=dim)
    return x


def scale_rows(values, gain):
    return values * lax.rsqrt(jnp.mean(values * values, axis=-1, keepdims=True) + epsilon) * gain


def project_all(normed, weights, products):
    result = []
    for member in range(len(weights)):
        if member < products:
            result.append(jnp.dot(normed, weights[member], preferred_element_type=jnp.float32))
        else:
            result.append(weights[member])
    return tuple(result)


def attention_branch(query, key, values, weight_two, query_gain, key_gain, head_gain):
    tok_rows = query.shape[0]
    vsize = head_gain.shape[0]
    half = query_gain.shape[0]
    heads = values.shape[1] // vsize
    query_normed = scale_rows(query.reshape(tok_rows, heads, 2, half), query_gain).astype(
        jnp.bfloat16
    )
    key_normed = scale_rows(key.reshape(tok_rows, heads * 2, half), key_gain).astype(jnp.bfloat16)
    key_normed = key_normed.reshape(tok_rows, heads * 2 * half)
    scale = half ** (-0.5)
    initial = (
        jnp.full((heads, 2, tok_rows), -1e30, jnp.float32),
        jnp.zeros((heads, 2, tok_rows), jnp.float32),
        jnp.zeros((heads, 2, tok_rows, vsize), jnp.float32),
    )
    carry = initial
    key_piece = lax.all_gather(key_normed, "sp", axis=0, tiled=True)
    value_piece = lax.all_gather(values, "sp", axis=0, tiled=True)
    length = key_piece.shape[0]
    block = math.gcd(length, 512)
    key_blocks = key_piece.reshape(length // block, block, heads, 2, half)
    value_blocks = value_piece.reshape(length // block, block, heads, vsize)

    def one_block(state, blocks):
        peak, total, accum = state
        key_block, value_block = blocks
        scores = (
            jnp.einsum(
                "qhjd,khjd->hjqk", query_normed, key_block, preferred_element_type=jnp.float32
            )
            * scale
        )
        new_peak = jnp.maximum(peak, jnp.max(scores, axis=-1))
        factor = jnp.exp(peak - new_peak)
        expo = jnp.exp(scores - new_peak[..., None])
        total = total * factor + jnp.sum(expo, axis=-1)
        accum = accum * factor[..., None] + jnp.einsum(
            "hjqk,khd->hjqd",
            expo.astype(jnp.bfloat16),
            value_block,
            preferred_element_type=jnp.float32,
        )
        return ((new_peak, total, accum), None)

    carry, unused = lax.scan(one_block, carry, (key_blocks, value_blocks))
    peak, total, accum = carry
    mapped = accum / total[..., None]
    head_out = mapped[:, 0] - weight_two[:, None, None] * mapped[:, 1]
    normed_out = scale_rows(head_out, head_gain).astype(jnp.bfloat16)
    return jnp.transpose(normed_out, (1, 0, 2)).reshape(tok_rows, heads * vsize)


def per_device(
    inputs,
    norm_gain,
    query_weight,
    key_weight,
    value_weight,
    query_gain,
    key_gain,
    mix_lambda,
    head_gain,
    post_gate_weight,
    pre_gate_weight,
    inner_weight,
    conv_taps,
    attn_out_weight,
    conv_out_weight,
):
    tokens = inputs[0]
    whole = lax.all_gather(tokens, "tp", axis=1, tiled=True)
    normed = scale_rows(whole.astype(jnp.float32), norm_gain).astype(jnp.bfloat16)
    heads_dev = value_weight.shape[1] // head_gain.shape[0]
    channels = post_gate_weight.shape[1]
    tp_index = lax.axis_index("tp")
    weight_two = lax.dynamic_slice_in_dim(mix_lambda, tp_index * heads_dev, heads_dev)
    taps = lax.dynamic_slice_in_dim(conv_taps, tp_index * channels, channels, 1)
    every_full = (
        lax.all_gather(query_weight, ("sp", "fs"), axis=0, tiled=True),
        lax.all_gather(key_weight, ("sp", "fs"), axis=0, tiled=True),
        lax.all_gather(value_weight, ("sp", "fs"), axis=0, tiled=True),
        lax.all_gather(post_gate_weight, ("sp", "fs"), axis=0, tiled=True),
        lax.all_gather(pre_gate_weight, ("sp", "fs"), axis=0, tiled=True),
        lax.all_gather(inner_weight, ("sp", "fs"), axis=0, tiled=True),
        lax.all_gather(attn_out_weight, ("sp", "fs"), axis=0, tiled=True),
        lax.all_gather(conv_out_weight, ("sp", "fs"), axis=0, tiled=True),
    )
    query, key, value_proj, post, pre_gate, inner, attn_out_full, conv_out_full = project_all(
        normed, every_full[0:3] + every_full[3:6] + every_full[6:8], 6
    )
    attn_hidden = attention_branch(
        query, key, value_proj.astype(jnp.bfloat16), weight_two, query_gain, key_gain, head_gain
    )
    post_mid = post.astype(jnp.bfloat16)
    post_wide = lax.optimization_barrier(post_mid).astype(jnp.float32)
    signal = (pre_gate * inner).astype(jnp.bfloat16)
    padded = padded_2(signal, (("sp", 0),), 1)
    shifted = lax.optimization_barrier(padded).astype(jnp.float32)
    filtered = taps[0] * shifted[:-2] + taps[1] * shifted[1:-1] + taps[2] * shifted[2:]
    conv_hidden = (post_wide * filtered).astype(jnp.bfloat16)
    contract = (((1,), (1,)), ((), ()))
    summed = lax.psum_scatter(
        (
            lax.dot_general(
                attn_hidden, attn_out_full, contract, preferred_element_type=jnp.float32
            )
            + lax.dot_general(
                conv_hidden, conv_out_full, contract, preferred_element_type=jnp.float32
            )
        ).astype(jnp.bfloat16),
        "tp",
        scatter_dimension=0,
        tiled=True,
    )
    return summed[None]


def solution(mesh):
    placed = (
        P("fs", "sp", "tp"),
        P(),
        P(("sp", "fs"), "tp"),
        P(("sp", "fs"), "tp"),
        P(("sp", "fs"), "tp"),
        P(),
        P(),
        P(),
        P(),
        P(("sp", "fs"), "tp"),
        P(("sp", "fs"), "tp"),
        P(("sp", "fs"), "tp"),
        P(),
        P(("sp", "fs"), "tp"),
        P(("sp", "fs"), "tp"),
    )
    return jax.shard_map(
        per_device,
        mesh=mesh,
        in_specs=placed,
        out_specs=P("fs", ("sp", "tp"), None),
        check_vma=False,
    )
```

profile of v0, /device:TPU:0, one launch (start us, length us, event | category | flops | bytes accessed | tf_op | source)
XLA Modules:
  0.0 693.1 jit_solution(11032667689516088220)
XLA Ops:
  10.1 12.1 %all-gather.33.cloned.1.call-done = bf16[1,512,2048]{2,1,0:T(8,128)(2,1)} async-done(((bf16[1,512,1024]{2,1,0:T(8,128)(2,1)}), bf16[1,512,2048]{2,1,0:T(8,128)(2,1)}) %all-gather.33.cloned.1.call-update) | async-done | bytes 2097168 | tf_op jit(solution)/shard_map/all_gather | solution.py:108
  24.4 62.1 %all-gather.13.cloned.1.call-done = bf16[2048,512]{1,0:T(8,128)(2,1)} async-done(((bf16[128,512]{1,0:T(8,128)(2,1)}), bf16[2048,512]{1,0:T(8,128)(2,1)}) %all-gather.13.cloned.1.call-update) | async-done | bytes 2097168 | tf_op jit(solution)/shard_map/all_gather | solution.py:117
  90.6 57.9 %all-gather.19.cloned.1.call-done = bf16[2048,512]{1,0:T(8,128)(2,1)} async-done(((bf16[128,512]{1,0:T(8,128)(2,1)}), bf16[2048,512]{1,0:T(8,128)(2,1)}) %all-gather.19.cloned.1.call-update) | async-done | bytes 2097168 | tf_op jit(solution)/shard_map/all_gather | solution.py:118
  157.1 53.3 %all-gather.17.cloned.1.call-done = bf16[2048,512]{1,0:T(8,128)(2,1)} async-done(((bf16[128,512]{1,0:T(8,128)(2,1)}), bf16[2048,512]{1,0:T(8,128)(2,1)}) %all-gather.17.cloned.1.call-update) | async-done | bytes 2097168 | tf_op jit(solution)/shard_map/all_gather | solution.py:116
  214.3 42.0 %all-gather.15.cloned.1.call-done = bf16[2048,512]{0,1:T(8,128)(2,1)} async-done(((bf16[512,512]{0,1:T(8,128)(2,1)}), bf16[2048,512]{0,1:T(8,128)(2,1)}) %all-gather.15.cloned.1.call-update) | async-done | bytes 2097168 | tf_op jit(solution)/shard_map/all_gather | solution.py:54
  264.2 38.0 %all-gather.21.cloned.1.call-done = bf16[2048,512]{1,0:T(8,128)(2,1)} async-done(((bf16[512,512]{1,0:T(8,128)(2,1)}), bf16[2048,512]{1,0:T(8,128)(2,1)}) %all-gather.21.cloned.1.call-update) | async-done | bytes 2097168 | tf_op jit(solution)/shard_map/all_gather | solution.py:55
  306.2 59.2 %while.15 = (s32[]{:T(128)}, f32[4,2,512]{2,1,0:T(2,128)S(1)}, f32[4,2,512]{2,1,0:T(2,128)S(1)}, f32[4,2,512,128]{3,2,1,0:T(8,128)S(1)}, bf16[4,512,4,2,64]{1,4,...) while((s32[]{:T(128)}, f32[4,2,512]{2,1,0:T(2,128)S(1)}, ...), condition=%wide.region_6.7_spmd.clone, body=%wide.region_3.6_spmd.clone.sunk | while | flops 823676928 | bytes 65798792 | solution.py:82
  306.2 5.6 bitcast_reduce_fusion.3
  311.9 5.1 fusion.62
  321.0 5.6 bitcast_reduce_fusion.3
  335.8 5.6 bitcast_reduce_fusion.3
  350.5 5.8 bitcast_reduce_fusion.3
  356.3 5.0 fusion.62
  370.1 9.3 %all-gather.27.cloned.1.call-done = bf16[2048,1024]{1,0:T(8,128)(2,1)} async-done(((bf16[128,1024]{1,0:T(8,128)(2,1)}), bf16[2048,1024]{1,0:T(8,128)(2,1)}) %all-gather.27.cloned.1.call-update) | async-done | bytes 4194320 | tf_op jit(solution)/shard_map/all_gather | solution.py:120
  379.4 5.9 fusion.34
  385.3 71.1 %all-gather.29.cloned.1.call-done = bf16[2048,1024]{1,0:T(8,128)(2,1)} async-done(((bf16[128,1024]{1,0:T(8,128)(2,1)}), bf16[2048,1024]{1,0:T(8,128)(2,1)}) %all-gather.29.cloned.1.call-update) | async-done | bytes 4194320 | tf_op jit(solution)/shard_map/all_gather | solution.py:121
  456.4 5.2 multiply_convert_fusion
  467.5 65.9 %all-gather.25.cloned.1.call-done = bf16[2048,1024]{1,0:T(8,128)(2,1)} async-done(((bf16[128,1024]{1,0:T(8,128)(2,1)}), bf16[2048,1024]{1,0:T(8,128)(2,1)}) %all-gather.25.cloned.1.call-update) | async-done | bytes 4194320 | tf_op jit(solution)/shard_map/all_gather | solution.py:119
  533.4 5.7 convolution_convert_fusion
  539.6 70.6 %all-gather.31.cloned.1.call-done = bf16[2048,1024]{1,0:T(8,128)(2,1)} async-done(((bf16[128,1024]{1,0:T(8,128)(2,1)}), bf16[2048,1024]{1,0:T(8,128)(2,1)}) %all-gather.31.cloned.1.call-update) | async-done | bytes 4194320 | tf_op jit(solution)/shard_map/all_gather | solution.py:123
  610.2 7.1 %fusion.24 = f32[512,2048]{1,0:T(8,128)} fusion(bf16[2048,1024]{1,0:T(8,128)(2,1)} %all-gather.31.cloned.1.call-done, f32[514,1024]{1,0:T(8,128)S(1)} %convert_element_type.49, bf16[512,1024]{1,0:T(8,128)(2,1)} %convolution_convert_fusion, f32[1024]{0:T(1024)S(1)} %bitcast.100, f32[1024]{0:T(1024)S(1)} %bitcast.99, f32[1024]{0:T(1024)S(1)} %bitcast.98), kind=kOutput, calls=%fused_computation.39 | convolution fusion | flops 2151677952 | bytes 15740928 | tf_op jit(solution)/shard_map/dot_general | solution.py:144
  617.4 54.7 %all-gather.23.cloned.1.call-done = bf16[2048,512]{1,0:T(8,128)(2,1)} async-done(((bf16[128,512]{1,0:T(8,128)(2,1)}), bf16[2048,512]{1,0:T(8,128)(2,1)}) %all-gather.23.cloned.1.call-update) | async-done | bytes 2097168 | tf_op jit(solution)/shard_map/all_gather | solution.py:122
  672.0 5.5 add_convert_fusion
  677.6 8.7 %reduce-scatter.2.cloned.1.call-done = bf16[256,2048]{1,0:T(8,128)(2,1)} async-done(((bf16[512,2048]{1,0:T(8,128)(2,1)}), bf16[256,2048]{1,0:T(8,128)(2,1)}) %reduce-scatter.2.cloned.1.call-update) | async-done | bytes 1048592 | tf_op jit(solution)/shard_map/reduce_scatter | solution.py:139
  (102 shorter events, 71.2 us)
Async XLA Ops:
  6.5 80.0 %copy-start.7 = (f32[2048]{0:T(1024)S(1)}, f32[2048]{0:T(1024)}, u32[]{:S(2)}) copy-start(f32[2048]{0:T(1024)} %param.18) | copy-start | bytes 24580
  6.5 15.7 %all-gather.33.cloned.1.call-start = ((), (), s32[]{:S(2)}) async-start(), calls=%async_computation.12 | async-start | bytes 3145728 | tf_op jit(solution)/shard_map/all_gather | solution.py:108
  7.3 79.3 %all-gather.13.cloned.1.call-start = ((), (), s32[]{:S(2)}) async-start(), calls=%async_computation.1 | async-start | bytes 2228224 | tf_op jit(solution)/shard_map/all_gather | solution.py:117
  8.0 140.5 %all-gather.19.cloned.1.call-start = ((), (), s32[]{:S(2)}) async-start(), calls=%async_computation.4 | async-start | bytes 2228224 | tf_op jit(solution)/shard_map/all_gather | solution.py:118
  8.7 201.6 %all-gather.17.cloned.1.call-start = ((), (), s32[]{:S(2)}) async-start(), calls=%async_computation.3 | async-start | bytes 2228224 | tf_op jit(solution)/shard_map/all_gather | solution.py:116
  9.3 247.0 %all-gather.15.cloned.1.call-start = ((), (), s32[]{:S(2)}) async-start(), calls=%async_computation.2 | async-start | bytes 2621440 | tf_op jit(solution)/shard_map/all_gather | solution.py:54
  22.2 64.4 %copy-start.1 = (bf16[1,512,2048]{2,1,0:T(8,128)(2,1)S(1)}, bf16[1,512,2048]{2,1,0:T(8,128)(2,1)}, u32[]{:S(2)}) copy-start(bf16[1,512,2048]{2,1,0:T(8,128)(2,1)} %all-gather.33.cloned.1.call-done) | copy-start | bytes 6291460
  90.6 65.5 %copy-start.8 = (f32[8]{0:T(128)S(1)}, f32[8]{0:T(128)}, u32[]{:S(2)}) copy-start(f32[8]{0:T(128)} %param.24) | copy-start | bytes 100
  90.6 211.6 %all-gather.21.cloned.1.call-start = ((), (), s32[]{:S(2)}) async-start(), calls=%async_computation.5 | async-start | bytes 2621440 | tf_op jit(solution)/shard_map/all_gather | solution.py:55
  152.3 227.1 %all-gather.27.cloned.1.call-start = ((), (), s32[]{:S(2)}) async-start(), calls=%async_computation.8 | async-start | bytes 4456448 | tf_op jit(solution)/shard_map/all_gather | solution.py:120
  153.0 303.4 %all-gather.29.cloned.1.call-start = ((), (), s32[]{:S(2)}) async-start(), calls=%async_computation.9 | async-start | bytes 4456448 | tf_op jit(solution)/shard_map/all_gather | solution.py:121
  153.8 379.6 %all-gather.25.cloned.1.call-start = ((), (), s32[]{:S(2)}) async-start(), calls=%async_computation.7 | async-start | bytes 4456448 | tf_op jit(solution)/shard_map/all_gather | solution.py:119
  154.5 455.7 %all-gather.31.cloned.1.call-start = ((), (), s32[]{:S(2)}) async-start(), calls=%async_computation.10 | async-start | bytes 4456448 | tf_op jit(solution)/shard_map/all_gather | solution.py:123
  155.1 516.9 %all-gather.23.cloned.1.call-start = ((), (), s32[]{:S(2)}) async-start(), calls=%async_computation.6 | async-start | bytes 2228224 | tf_op jit(solution)/shard_map/all_gather | solution.py:122
  155.8 530.4 %reduce-scatter.2.cloned.1.call-start = ((), (), s32[]{:S(2)}) async-start(), calls=%async_computation.11 | async-start | bytes 3145728 | tf_op jit(solution)/shard_map/reduce_scatter | solution.py:139
  157.1 57.0 %copy-start.5 = (f32[64]{0:T(128)S(1)}, f32[64]{0:T(128)}, u32[]{:S(2)}) copy-start(f32[64]{0:T(128)} %param.22) | copy-start | bytes 772
  311.8 6.4 copy-start
  326.7 6.3 copy-start
  341.4 6.3 copy-start
  356.3 6.3 copy-start
  369.2 10.2 %copy-start.2 = (bf16[1,512,2048]{2,1,0:T(8,128)(2,1)S(1)}, bf16[1,512,2048]{2,1,0:T(8,128)(2,1)}, u32[]{:S(2)}) copy-start(bf16[1,512,2048]{2,1,0:T(8,128)(2,1)} %all-gather.33.cloned.1.call-done) | copy-start | bytes 6291460
  462.6 76.5 %collective-permute-start = (bf16[1,1024]{1,0:T(2,128)(2,1)S(1)}, bf16[1,1024]{1,0:T(2,128)(2,1)S(1)}, u32[]{:S(2)}, u32[]{:S(2)}) collective-permute-start(bf16[1,1024]{1,0:T(2,128)(2,1)S(1)} %get-tuple-element.101), channel_id=1, source_target_pairs={{0,8},{8,16},{16,24},{1,9},{9,17},{17,25},{2,10},{10,18},{18,26},{... | collective-permute-start | bytes 6152 | tf_op jit(solution)/shard_map/ppermute | solution.py:17
  466.0 73.1 %collective-permute-start.1 = (bf16[1,1024]{1,0:T(2,128)(2,1)S(1)}, bf16[1,1024]{1,0:T(2,128)(2,1)S(1)}, u32[]{:S(2)}, u32[]{:S(2)}) collective-permute-start(bf16[1,1024]{1,0:T(2,128)(2,1)S(1)} %get-tuple-element.102), channel_id=1, source_target_pairs={{8,0},{16,8},{24,16},{9,1},{17,9},{25,17},{10,2},{18,10},{26,18},{... | collective-permute-start | bytes 6152 | tf_op jit(solution)/shard_map/ppermute | solution.py:18
  533.4 5.7 copy-start.4
  (2 other events, 1.6 us)
Sparse Core Ops, SparseCore 0:
  8.9 13.2 all-gather.32
  25.0 61.5 all-gather.12
  89.3 59.1 all-gather.18
  151.2 59.1 all-gather.16
  211.8 44.4 all-gather.14
  257.7 44.4 all-gather.20
  305.0 74.3 all-gather.26
  382.2 74.1 all-gather.28
  459.2 74.1 all-gather.24
  536.0 74.1 all-gather.30
  613.0 58.9 all-gather.22
  677.7 8.5 reduce-scatter.1
where the time goes:
time: 694 us; the launch traced here: 693 us
  waiting for transfers between devices  552 us (80%)
  matrix products  73.6 us (11%)
  other arithmetic  26.6 us (4%)
  local copies, waits for them, and re-layouts  21.7 us (3%)
  between operations  13.8 us (2%)
    all_gather x1, waiting for transfers between devices, per_device(): lax.all_gather(inner_weight, ('sp', 'fs'), axis=0, tiled=True)  71.1 us
    all_gather x1, waiting for transfers between devices, per_device(): lax.all_gather(conv_out_weight, ('sp', 'fs'), axis=0, tiled=True)  70.6 us
    all_gather x1, waiting for transfers between devices, per_device(): lax.all_gather(post_gate_weight, ('sp', 'fs'), axis=0, tiled=True)  65.9 us
    all_gather x1, waiting for transfers between devices, per_device(): lax.all_gather(key_weight, ('sp', 'fs'), axis=0, tiled=True)  62.1 us
    all_gather x1, waiting for transfers between devices, per_device(): lax.all_gather(value_weight, ('sp', 'fs'), axis=0, tiled=True)  57.9 us
    all_gather x1, waiting for transfers between devices, per_device(): lax.all_gather(attn_out_weight, ('sp', 'fs'), axis=0, tiled=True)  54.7 us
    all_gather x1, waiting for transfers between devices, per_device(): lax.all_gather(query_weight, ('sp', 'fs'), axis=0, tiled=True)  53.3 us
    all_gather x1, waiting for transfers between devices, attention_branch(): key_piece = lax.all_gather(key_normed, 'sp', axis=0, tiled=True)  42 us
  transfers between devices with their start and end apart: 14, of which 12 were waited for; matrix products, arithmetic and copies ran while one was open for 17% of the time, Pallas kernels for 0%

commit v1 on v0

--- a/solution.py
+++ b/solution.py
@@ -52,7 +52,14 @@
     )
     carry = initial
     key_piece = lax.all_gather(key_normed, "sp", axis=0, tiled=True)
-    value_piece = lax.all_gather(values, "sp", axis=0, tiled=True)
+    peers = lax.axis_size("sp")
+    route = [(i_2, (i_2 + 1) % peers) for i_2 in range(peers)]
+    parts = [values]
+    for far in range(1, peers):
+        parts = [lax.ppermute(parts[0], "sp", route), *parts]
+    full = jnp.concatenate(parts, axis=0)
+    places = (lax.axis_index("sp") + 1) * parts[-1].shape[0]
+    value_piece = jnp.roll(full, places, axis=0)
     length = key_piece.shape[0]
     block = math.gcd(length, 512)
     key_blocks = key_piece.reshape(length // block, block, heads, 2, half)

time: 694 us -> 658 us (0.948)
  waiting for transfers between devices: 552 us -> 509 us
    all_gather x1 -> x0, waiting for transfers between devices: 38 us -> none  [attention_branch(): value_piece = lax.all_gather(values, 'sp', axis=0, tiled=True)]
    ppermute x0 -> x3, waiting for transfers between devices: none -> 27.2 us  [attention_branch(): parts = [lax.ppermute(parts[0], 'sp', route), *parts]]
    all_gather x1, waiting for transfers between devices: 53.3 us -> 39.4 us  [per_device(): lax.all_gather(query_weight, ('sp', 'fs'), axis=0, tiled=True)]
    all_gather x1, waiting for transfers between devices: 42 us -> 31.9 us  [attention_branch(): key_piece = lax.all_gather(key_normed, 'sp', axis=0, tiled=True)]
  transfers between devices with their start and end apart: 14 -> 16, of which waited for: 12 -> 13; matrix products, arithmetic and copies ran while one was open for 17% -> 18% of each run, Pallas kernels for 0% -> 0%
where the time goes in v1:
time: 658 us; the launch traced here: 657 us
  waiting for transfers between devices  509 us (77%)
  matrix products  73.3 us (11%)
  local copies, waits for them, and re-layouts  27.5 us (4%)
  other arithmetic  26.4 us (4%)
  between operations  13.6 us (2%)
  starting transfers between devices  6.83 us (1%)
    all_gather x1, waiting for transfers between devices, per_device(): lax.all_gather(inner_weight, ('sp', 'fs'), axis=0, tiled=True)  71.1 us
    all_gather x1, waiting for transfers between devices, per_device(): lax.all_gather(conv_out_weight, ('sp', 'fs'), axis=0, tiled=True)  70.7 us
    all_gather x1, waiting for transfers between devices, per_device(): lax.all_gather(post_gate_weight, ('sp', 'fs'), axis=0, tiled=True)  65.8 us
    all_gather x1, waiting for transfers between devices, per_device(): lax.all_gather(key_weight, ('sp', 'fs'), axis=0, tiled=True)  62.3 us
    all_gather x1, waiting for transfers between devices, per_device(): lax.all_gather(attn_out_weight, ('sp', 'fs'), axis=0, tiled=True)  54.5 us
    all_gather x1, waiting for transfers between devices, per_device(): lax.all_gather(value_weight, ('sp', 'fs'), axis=0, tiled=True)  54.5 us
    all_gather x1, waiting for transfers between devices, per_device(): lax.all_gather(query_weight, ('sp', 'fs'), axis=0, tiled=True)  39.4 us
    all_gather x1, waiting for transfers between devices, attention_branch(): key_piece = lax.all_gather(key_normed, 'sp', axis=0, tiled=True)  31.9 us
  transfers between devices with their start and end apart: 16, of which 13 were waited for; matrix products, arithmetic and copies ran while one was open for 18% of the time, Pallas kernels for 0%

profile of v1, /device:TPU:0, one launch (start us, length us, event | category | flops | bytes accessed | tf_op | source)
XLA Modules:
  0.0 657.0 jit_solution(12323183303610203938)
XLA Ops:
  10.1 12.1 %all-gather.30.cloned.1.call-done = bf16[1,512,2048]{2,1,0:T(8,128)(2,1)} async-done(((bf16[1,512,1024]{2,1,0:T(8,128)(2,1)}), bf16[1,512,2048]{2,1,0:T(8,128)(2,1)}) %all-gather.30.cloned.1.call-update) | async-done | bytes 2097168 | tf_op jit(solution)/shard_map/all_gather | solution.py:115
  24.3 62.3 %all-gather.12.cloned.1.call-done = bf16[2048,512]{1,0:T(8,128)(2,1)} async-done(((bf16[128,512]{1,0:T(8,128)(2,1)}), bf16[2048,512]{1,0:T(8,128)(2,1)}) %all-gather.12.cloned.1.call-update) | async-done | bytes 2097168 | tf_op jit(solution)/shard_map/all_gather | solution.py:124
  94.1 54.5 %all-gather.18.cloned.1.call-done = bf16[2048,512]{1,0:T(8,128)(2,1)} async-done(((bf16[128,512]{1,0:T(8,128)(2,1)}), bf16[2048,512]{1,0:T(8,128)(2,1)}) %all-gather.18.cloned.1.call-update) | async-done | bytes 2097168 | tf_op jit(solution)/shard_map/all_gather | solution.py:125
  153.0 14.8 %collective-permute-done = bf16[512,512]{1,0:T(8,128)(2,1)S(1)} collective-permute-done((bf16[512,512]{1,0:T(8,128)(2,1)S(1)}, bf16[512,512]{1,0:T(8,128)(2,1)S(1)}, u32[]{:S(2)}, u32[]{:S(2)}) %collective-permute-start) | collective-permute-done | bytes 524320 | tf_op jit(solution)/shard_map/ppermute | solution.py:59
  168.9 12.4 %collective-permute-done.1 = bf16[512,512]{1,0:T(8,128)(2,1)} collective-permute-done((bf16[512,512]{1,0:T(8,128)(2,1)S(1)}, bf16[512,512]{1,0:T(8,128)(2,1)}, u32[]{:S(2)}, u32[]{:S(2)}) %collective-permute-start.1) | collective-permute-done | bytes 524320 | tf_op jit(solution)/shard_map/ppermute | solution.py:59
  181.3 39.4 %all-gather.16.cloned.1.call-done = bf16[2048,512]{1,0:T(8,128)(2,1)} async-done(((bf16[128,512]{1,0:T(8,128)(2,1)}), bf16[2048,512]{1,0:T(8,128)(2,1)}) %all-gather.16.cloned.1.call-update) | async-done | bytes 2097168 | tf_op jit(solution)/shard_map/all_gather | solution.py:123
  234.7 31.9 %all-gather.14.cloned.1.call-done = bf16[2048,512]{0,1:T(8,128)(2,1)} async-done(((bf16[512,512]{0,1:T(8,128)(2,1)}), bf16[2048,512]{0,1:T(8,128)(2,1)}) %all-gather.14.cloned.1.call-update) | async-done | bytes 2097168 | tf_op jit(solution)/shard_map/all_gather | solution.py:54
  274.5 59.0 %while.15 = (s32[]{:T(128)}, f32[4,2,512]{2,1,0:T(2,128)S(1)}, f32[4,2,512]{2,1,0:T(2,128)S(1)}, f32[4,2,512,128]{3,2,1,0:T(8,128)S(1)}, bf16[4,512,4,2,64]{1,4,...) while((s32[]{:T(128)}, f32[4,2,512]{2,1,0:T(2,128)S(1)}, ...), condition=%wide.region_6.7_spmd.clone, body=%wide.region_3.6_spmd.clone.sunk | while | flops 823676928 | bytes 65798792 | solution.py:89
  274.5 5.6 bitcast_reduce_fusion.3
  280.1 5.0 fusion.62
  289.3 5.6 bitcast_reduce_fusion.3
  304.0 5.6 bitcast_reduce_fusion.3
  318.8 5.6 bitcast_reduce_fusion.3
  337.8 5.8 all-gather.24.cloned.1.call-done
  343.7 5.9 fusion.34
  349.6 71.1 %all-gather.26.cloned.1.call-done = bf16[2048,1024]{1,0:T(8,128)(2,1)} async-done(((bf16[128,1024]{1,0:T(8,128)(2,1)}), bf16[2048,1024]{1,0:T(8,128)(2,1)}) %all-gather.26.cloned.1.call-update) | async-done | bytes 4194320 | tf_op jit(solution)/shard_map/all_gather | solution.py:128
  420.7 5.2 multiply_convert_fusion
  431.8 65.8 %all-gather.22.cloned.1.call-done = bf16[2048,1024]{1,0:T(8,128)(2,1)} async-done(((bf16[128,1024]{1,0:T(8,128)(2,1)}), bf16[2048,1024]{1,0:T(8,128)(2,1)}) %all-gather.22.cloned.1.call-update) | async-done | bytes 4194320 | tf_op jit(solution)/shard_map/all_gather | solution.py:126
  497.6 5.7 convolution_convert_fusion
  503.9 70.7 %all-gather.28.cloned.1.call-done = bf16[2048,1024]{1,0:T(8,128)(2,1)} async-done(((bf16[128,1024]{1,0:T(8,128)(2,1)}), bf16[2048,1024]{1,0:T(8,128)(2,1)}) %all-gather.28.cloned.1.call-update) | async-done | bytes 4194320 | tf_op jit(solution)/shard_map/all_gather | solution.py:130
  574.6 7.1 %fusion.24 = f32[512,2048]{1,0:T(8,128)} fusion(bf16[2048,1024]{1,0:T(8,128)(2,1)} %all-gather.28.cloned.1.call-done, f32[514,1024]{1,0:T(8,128)S(1)} %convert_element_type.49, bf16[512,1024]{1,0:T(8,128)(2,1)} %convolution_convert_fusion, f32[1024]{0:T(1024)S(1)} %bitcast.100, f32[1024]{0:T(1024)S(1)} %bitcast.99, f32[1024]{0:T(1024)S(1)} %bitcast.98), kind=kOutput, calls=%fused_computation.39 | convolution fusion | flops 2151677952 | bytes 15740928 | tf_op jit(solution)/shard_map/dot_general | solution.py:151
  581.8 54.5 %all-gather.20.cloned.1.call-done = bf16[2048,512]{1,0:T(8,128)(2,1)} async-done(((bf16[128,512]{1,0:T(8,128)(2,1)}), bf16[2048,512]{1,0:T(8,128)(2,1)}) %all-gather.20.cloned.1.call-update) | async-done | bytes 2097168 | tf_op jit(solution)/shard_map/all_gather | solution.py:129
  636.3 5.5 add_convert_fusion
  641.8 8.7 %reduce-scatter.2.cloned.1.call-done = bf16[256,2048]{1,0:T(8,128)(2,1)} async-done(((bf16[512,2048]{1,0:T(8,128)(2,1)}), bf16[256,2048]{1,0:T(8,128)(2,1)}) %reduce-scatter.2.cloned.1.call-update) | async-done | bytes 1048592 | tf_op jit(solution)/shard_map/reduce_scatter | solution.py:146
  (118 shorter events, 82.3 us)
Async XLA Ops:
  6.5 80.0 %copy-start.9 = (f32[2048]{0:T(1024)S(1)}, f32[2048]{0:T(1024)}, u32[]{:S(2)}) copy-start(f32[2048]{0:T(1024)} %param.18) | copy-start | bytes 24580
  6.5 15.7 %all-gather.30.cloned.1.call-start = ((), (), s32[]{:S(2)}) async-start(), calls=%async_computation.11 | async-start | bytes 3145728 | tf_op jit(solution)/shard_map/all_gather | solution.py:115
  7.3 79.3 %all-gather.12.cloned.1.call-start = ((), (), s32[]{:S(2)}) async-start(), calls=%async_computation.1 | async-start | bytes 2228224 | tf_op jit(solution)/shard_map/all_gather | solution.py:124
  8.0 140.5 %all-gather.18.cloned.1.call-start = ((), (), s32[]{:S(2)}) async-start(), calls=%async_computation.4 | async-start | bytes 2228224 | tf_op jit(solution)/shard_map/all_gather | solution.py:125
  8.7 212.0 %all-gather.16.cloned.1.call-start = ((), (), s32[]{:S(2)}) async-start(), calls=%async_computation.3 | async-start | bytes 2228224 | tf_op jit(solution)/shard_map/all_gather | solution.py:123
  9.3 257.3 %all-gather.14.cloned.1.call-start = ((), (), s32[]{:S(2)}) async-start(), calls=%async_computation.2 | async-start | bytes 2621440 | tf_op jit(solution)/shard_map/all_gather | solution.py:54
  90.2 58.4 %copy-start.1 = (bf16[1,512,2048]{2,1,0:T(8,128)(2,1)S(1)}, bf16[1,512,2048]{2,1,0:T(8,128)(2,1)}, u32[]{:S(2)}) copy-start(bf16[1,512,2048]{2,1,0:T(8,128)(2,1)} %all-gather.30.cloned.1.call-done) | copy-start | bytes 6291460
  91.2 252.5 %all-gather.24.cloned.1.call-start = ((), (), s32[]{:S(2)}) async-start(), calls=%async_computation.7 | async-start | bytes 4456448 | tf_op jit(solution)/shard_map/all_gather | solution.py:127
  91.8 328.9 %all-gather.26.cloned.1.call-start = ((), (), s32[]{:S(2)}) async-start(), calls=%async_computation.8 | async-start | bytes 4456448 | tf_op jit(solution)/shard_map/all_gather | solution.py:128
  92.5 405.1 %all-gather.22.cloned.1.call-start = ((), (), s32[]{:S(2)}) async-start(), calls=%async_computation.6 | async-start | bytes 4456448 | tf_op jit(solution)/shard_map/all_gather | solution.py:126
  93.3 481.4 %all-gather.28.cloned.1.call-start = ((), (), s32[]{:S(2)}) async-start(), calls=%async_computation.9 | async-start | bytes 4456448 | tf_op jit(solution)/shard_map/all_gather | solution.py:130
  94.0 73.9 %copy-start.10 = (f32[8]{0:T(128)S(1)}, f32[8]{0:T(128)}, u32[]{:S(2)}) copy-start(f32[8]{0:T(128)} %param.24) | copy-start | bytes 100
  94.0 542.3 %all-gather.20.cloned.1.call-start = ((), (), s32[]{:S(2)}) async-start(), calls=%async_computation.5 | async-start | bytes 2228224 | tf_op jit(solution)/shard_map/all_gather | solution.py:129
  151.4 16.3 %collective-permute-start = (bf16[512,512]{1,0:T(8,128)(2,1)S(1)}, bf16[512,512]{1,0:T(8,128)(2,1)S(1)}, u32[]{:S(2)}, u32[]{:S(2)}) collective-permute-start(bf16[512,512]{1,0:T(8,128)(2,1)S(1)} %convolution_convert_fusion.1), channel_id=1, source_target_pairs={{0,8},{8,16},{16,24},{24,0},{1,9},{9,17},{17,25},{25,1},{2,10},{10... | collective-permute-start | bytes 1572872 | tf_op jit(solution)/shard_map/ppermute | solution.py:59
  167.7 56.6 %copy-start.3 = (bf16[512,512]{1,0:T(8,128)(2,1)}, bf16[512,512]{1,0:T(8,128)(2,1)S(1)}, u32[]{:S(2)}) copy-start(bf16[512,512]{1,0:T(8,128)(2,1)S(1)} %collective-permute-done) | copy-start | bytes 1572868
  167.7 13.6 %collective-permute-start.1 = (bf16[512,512]{1,0:T(8,128)(2,1)S(1)}, bf16[512,512]{1,0:T(8,128)(2,1)}, u32[]{:S(2)}, u32[]{:S(2)}) collective-permute-start(bf16[512,512]{1,0:T(8,128)(2,1)S(1)} %collective-permute-done), channel_id=1, source_target_pairs={{0,8},{8,16},{16,24},{24,0},{1,9},{9,17},{17,25},{25,1},{2,10},{10... | collective-permute-start | bytes 1572872 | tf_op jit(solution)/shard_map/ppermute | solution.py:59
  167.8 482.8 %reduce-scatter.2.cloned.1.call-start = ((), (), s32[]{:S(2)}) async-start(), calls=%async_computation.10 | async-start | bytes 3145728 | tf_op jit(solution)/shard_map/reduce_scatter | solution.py:146
  168.9 55.5 %copy-start.7 = (f32[64]{0:T(128)S(1)}, f32[64]{0:T(128)}, u32[]{:S(2)}) copy-start(f32[64]{0:T(128)} %param.22) | copy-start | bytes 772
  181.3 43.3 %collective-permute-start.2 = (bf16[512,512]{1,0:T(8,128)(2,1)}, bf16[512,512]{1,0:T(8,128)(2,1)}, u32[]{:S(2)}, u32[]{:S(2)}) collective-permute-start(bf16[512,512]{1,0:T(8,128)(2,1)} %collective-permute-done.1), channel_id=1, source_target_pairs={{0,8},{8,16},{16,24},{24,0},{1,9},{9,17},{17,25},{25,1},{2,10},{10... | collective-permute-start | bytes 1572872 | tf_op jit(solution)/shard_map/ppermute | solution.py:59
  280.1 6.3 copy-start
  324.4 6.3 copy-start
  337.2 6.4 copy-start.2
  426.9 76.5 %collective-permute-start.3 = (bf16[1,1024]{1,0:T(2,128)(2,1)S(1)}, bf16[1,1024]{1,0:T(2,128)(2,1)S(1)}, u32[]{:S(2)}, u32[]{:S(2)}) collective-permute-start(bf16[1,1024]{1,0:T(2,128)(2,1)S(1)} %get-tuple-element.101), channel_id=1, source_target_pairs={{0,8},{8,16},{16,24},{1,9},{9,17},{17,25},{2,10},{10,18},{18,26},{... | collective-permute-start | bytes 6152 | tf_op jit(solution)/shard_map/ppermute | solution.py:17
  430.3 73.1 %collective-permute-start.4 = (bf16[1,1024]{1,0:T(2,128)(2,1)S(1)}, bf16[1,1024]{1,0:T(2,128)(2,1)S(1)}, u32[]{:S(2)}, u32[]{:S(2)}) collective-permute-start(bf16[1,1024]{1,0:T(2,128)(2,1)S(1)} %get-tuple-element.102), channel_id=1, source_target_pairs={{8,0},{16,8},{24,16},{9,1},{17,9},{25,17},{10,2},{18,10},{26,18},{... | collective-permute-start | bytes 6152 | tf_op jit(solution)/shard_map/ppermute | solution.py:18
  (6 other events, 23.9 us)
Sparse Core Ops, SparseCore 0:
  8.9 13.2 all-gather.29
  25.0 61.5 all-gather.11
  89.3 59.1 all-gather.17
  151.2 69.4 all-gather.15
  222.1 44.4 all-gather.13
  269.2 74.3 all-gather.23
  346.4 74.1 all-gather.25
  423.4 74.1 all-gather.21
  500.4 74.1 all-gather.27
  577.3 58.9 all-gather.19
  641.9 8.5 reduce-scatter.1
